TPU v7x, 32 devices: a whole 2x2x4 slice. The times are simulated.
32 devices in a mesh: fs: 8 (over z, x), tp: 4 (over y, core).
Axes of the slice: x: 2, y: 2, z: 4, core: 2. Of those that a mesh axis runs over, the one named last changes fastest.
Arguments:
- tokens: bfloat16 [4096, 2048], P('fs', 'tp'), may hold values from -6 to 6
- pre_gain: float32 [2048], P('fs'), may hold values from 0.1 to 1.9
- gate_weight: float32 [2048, 6144], P('fs', 'tp'), may hold values from -0.125 to 0.125
- up_weight: float32 [2048, 6144], P('fs', 'tp'), may hold values from -0.125 to 0.125
- down_weight: float32 [2048, 6144], P('fs', 'tp'), may hold values from -0.078125 to 0.078125
- post_gain: float32 [2048], P('tp'), may hold values from 0.1 to 1.9
Outputs:
- result: bfloat16 [4096, 2048], P('fs', 'tp')
- gate_ready: bfloat16 [2048, 6144], P(None, 'tp')
- up_ready: bfloat16 [2048, 6144], P(None, 'tp')
- down_ready: bfloat16 [2048, 6144], P(None, 'tp')
All inputs are finite; a program needn't handle non-finite values.
Results may differ from a plain program's by a relative error of at most 0.015.
Values may be sent and summed in bfloat16 or wider, within the bound.
A program may use at most 128 MiB of HBM per device.

v0:
```python
import jax
import jax.numpy as jnp
from jax import lax
from jax.sharding import PartitionSpec as P

EPS = 1e-06


def shards(tokens, pre_gain, gate_weight, up_weight, down_weight, post_gain):
    gate_local = (pre_gain[:, None] * gate_weight).astype(jnp.bfloat16)
    up_local = (pre_gain[:, None] * up_weight).astype(jnp.bfloat16)
    down_local = down_weight.astype(jnp.bfloat16)
    whole = lax.all_gather(tokens, "tp", axis=1, tiled=True)
    widened = whole.astype(jnp.float32)
    width = whole.shape[1]
    normalized = (
        widened * lax.rsqrt(jnp.mean(widened * widened, axis=1, keepdims=True) + EPS)
    ).astype(jnp.bfloat16)
    contract = (((1,), (1,)), ((), ()))
    gate_full, up_full, down_full = (
        lax.all_gather(gate_local, "fs", axis=0, tiled=True),
        lax.all_gather(up_local, "fs", axis=0, tiled=True),
        lax.all_gather(down_local, "fs", axis=0, tiled=True),
    )
    gate = jnp.dot(normalized, gate_full, preferred_element_type=jnp.float32)
    up = jnp.dot(normalized, up_full, preferred_element_type=jnp.float32)
    hidden = (jax.nn.silu(gate) * up).astype(jnp.bfloat16)
    partial_value = lax.dot_general(hidden, down_full, contract, preferred_element_type=jnp.float32)
    share = lax.psum_scatter(
        partial_value.astype(jnp.bfloat16), "tp", scatter_dimension=1, tiled=True
    ).astype(jnp.float32)
    squares = lax.psum(jnp.sum(share * share, axis=1, keepdims=True), "tp")
    scaling = lax.rsqrt(squares / width + EPS)
    result = (share * scaling * post_gain[None, :]).astype(jnp.bfloat16)
    return (result, gate_full, up_full, down_full)


def solution(mesh):
    return jax.shard_map(
        shards,
        mesh=mesh,
        in_specs=(P("fs", "tp"), P("fs"), P("fs", "tp"), P("fs", "tp"), P("fs", "tp"), P("tp")),
        out_specs=(P("fs", "tp"), P(None, "tp"), P(None, "tp"), P(None, "tp")),
        check_vma=False,
    )
```

profile of v0, /device:TPU:0, one launch (start us, length us, event | category | flops | bytes accessed | tf_op | source)
XLA Modules:
  0.0 406.3 jit_solution(389480162345285521)
XLA Ops:
  7.2 0.0 all-gather.5.cloned.1.call-start
  7.2 0.7 all-gather.5.cloned.1.call-update
  7.9 0.0 copy-start.1
  7.9 0.0 all-gather.7.cloned.1.call-start
  8.0 3.5 multiply_convert_fusion.1
  11.5 0.0 all-gather.7.cloned.1.call-update
  11.5 0.0 all-gather.9.cloned.1.call-start
  11.6 0.7 all-gather.9.cloned.1.call-update
  12.3 0.0 all-gather.11.cloned.1.call-start
  12.3 0.0 copy-done.1
  12.3 1.0 convert_element_type.32
  13.3 0.0 all-gather.11.cloned.1.call-update
  13.3 0.0 reduce-scatter.2.cloned.1.call-start
  13.4 21.5 %all-gather.5.cloned.1.call-done = bf16[512,2048]{1,0:T(8,128)(2,1)} async-done(((bf16[512,512]{1,0:T(8,128)(2,1)}), bf16[512,2048]{1,0:T(8,128)(2,1)}) %all-gather.5.cloned.1.call-update) | async-done | bytes 2097168 | tf_op jit(solution)/shard_map/all_gather | solution.py:13
  34.9 2.1 fusion
  36.9 0.0 copy-start
  37.0 99.4 %all-gather.7.cloned.1.call-done = bf16[2048,1536]{1,0:T(8,128)(2,1)} async-done(((bf16[256,1536]{1,0:T(8,128)(2,1)}), bf16[2048,1536]{1,0:T(8,128)(2,1)}) %all-gather.7.cloned.1.call-update) | async-done | bytes 6291472 | tf_op jit(solution)/shard_map/all_gather | solution.py:21
  136.3 8.5 %fusion.7 = f32[512,1536]{1,0:T(8,128)} fusion(bf16[2048,1536]{1,0:T(8,128)(2,1)} %all-gather.7.cloned.1.call-done, bf16[512,2048]{1,0:T(8,128)(2,1)} %all-gather.5.cloned.1.call-done, f32[512]{0:T(512)S(1)} %add_rsqrt_fusion.1), kind=kOutput, calls=%fused_computation.14 | convolution fusion | flops 3224371200 | bytes 11536384 | tf_op jit(solution)/shard_map/dot_general | solution.py:25
  144.9 0.0 copy-start.2
  144.9 91.1 %all-gather.9.cloned.1.call-done = bf16[2048,1536]{1,0:T(8,128)(2,1)} async-done(((bf16[256,1536]{1,0:T(8,128)(2,1)}), bf16[2048,1536]{1,0:T(8,128)(2,1)}) %all-gather.9.cloned.1.call-update) | async-done | bytes 6291472 | tf_op jit(solution)/shard_map/all_gather | solution.py:22
  236.0 99.5 %all-gather.11.cloned.1.call-done = bf16[2048,1536]{1,0:T(8,128)(2,1)} async-done(((bf16[256,1536]{1,0:T(8,128)(2,1)}), bf16[2048,1536]{1,0:T(8,128)(2,1)}) %all-gather.11.cloned.1.call-update) | async-done | bytes 6291472 | tf_op jit(solution)/shard_map/all_gather | solution.py:23
  335.5 0.0 copy-done
  335.5 13.6 %convolution_convert_fusion = bf16[512,2048]{1,0:T(8,128)(2,1)} fusion(bf16[2048,1536]{1,0:T(8,128)(2,1)} %all-gather.11.cloned.1.call-done, bf16[2048,1536]{1,0:T(8,128)(2,1)} %all-gather.9.cloned.1.call-done, f32[512,1536]{1,0:T(8,128)} %fusion.7, bf16[512,2048]{1,0:T(8,128)(2,1)S(1)} %copy-done, f32[512]{0:T(512)S(1)} %add_rsqrt_fusion.1), kind=kOutput, calls=%fused_computation.6 | convolution fusion | flops 6451363840 | bytes 19924992 | tf_op jit(solution)/shard_map/dot_general | solution.py:28
  349.2 0.0 reduce-scatter.2.cloned.1.call-update
  349.2 29.5 %reduce-scatter.2.cloned.1.call-done = bf16[512,512]{1,0:T(8,128)(2,1)} async-done(((bf16[512,2048]{1,0:T(8,128)(2,1)}), bf16[512,512]{1,0:T(8,128)(2,1)}) %reduce-scatter.2.cloned.1.call-update) | async-done | bytes 524304 | tf_op jit(solution)/shard_map/reduce_scatter | solution.py:29
  378.7 1.2 fusion.3
  379.9 5.8 %psum.7 = f32[512,1]{0,1:T(1,128)S(1)} all-reduce(f32[512,1]{0,1:T(1,128)S(1)} %bitcast.10), channel_id=1, replica_groups=mesh['fs'=8,'tp'=4] {'tp'}, use_global_device_ids=true, to_apply=%region_3.4 | all-reduce | flops 512 | bytes 4096 | tf_op jit(solution)/shard_map/psum | solution.py:32
  385.7 0.0 copy-done.2
  385.7 0.0 slice-start
  385.7 2.2 fusion.5
  387.8 0.0 slice-start.1
  387.8 0.0 slice-start.2
  387.8 6.1 %copy.13 = bf16[2048,1536]{1,0:T(8,128)(2,1)} copy(bf16[2048,1536]{1,0:T(8,128)(2,1)} %all-gather.7.cloned.1.call-done) | data formatting | bytes 12582912
  393.9 0.0 slice-done
  393.9 0.0 slice-done.1
  393.9 0.0 slice-start.3
  393.9 2.8 copy.14
  396.8 0.0 slice-done.2
  396.8 0.3 slice-done.3
  397.0 2.7 copy.15
  (4 shorter events, 0.0 us)
Async XLA Ops:
  7.2 27.7 %all-gather.5.cloned.1.call-start = ((), (), s32[]{:S(2)}) async-start(), calls=%async_computation.1 | async-start | bytes 2621440 | tf_op jit(solution)/shard_map/all_gather | solution.py:13
  7.9 4.4 %copy-start.1 = (f32[256,1536]{1,0:T(8,128)S(1)}, f32[256,1536]{1,0:T(8,128)}, u32[]{:S(2)}) copy-start(f32[256,1536]{1,0:T(8,128)} %param.10) | copy-start | bytes 4718596
  7.9 128.4 %all-gather.7.cloned.1.call-start = ((), (), s32[]{:S(2)}) async-start(), calls=%async_computation.2 | async-start | bytes 7077888 | tf_op jit(solution)/shard_map/all_gather | solution.py:21
  11.5 224.5 %all-gather.9.cloned.1.call-start = ((), (), s32[]{:S(2)}) async-start(), calls=%async_computation.3 | async-start | bytes 7077888 | tf_op jit(solution)/shard_map/all_gather | solution.py:22
  12.3 323.3 %all-gather.11.cloned.1.call-start = ((), (), s32[]{:S(2)}) async-start(), calls=%async_computation.4 | async-start | bytes 7077888 | tf_op jit(solution)/shard_map/all_gather | solution.py:23
  13.3 365.4 %reduce-scatter.2.cloned.1.call-start = ((), (), s32[]{:S(2)}) async-start(), calls=%async_computation.5 | async-start | bytes 2621440 | tf_op jit(solution)/shard_map/reduce_scatter | solution.py:29
  36.9 298.6 %copy-start = (bf16[512,2048]{1,0:T(8,128)(2,1)S(1)}, bf16[512,2048]{1,0:T(8,128)(2,1)}, u32[]{:S(2)}) copy-start(bf16[512,2048]{1,0:T(8,128)(2,1)} %all-gather.5.cloned.1.call-done) | copy-start | bytes 6291460
  144.9 240.8 %copy-start.2 = (f32[512]{0:T(512)S(1)}, f32[512]{0:T(512)}, u32[]{:S(2)}) copy-start(f32[512]{0:T(512)} %param.11) | copy-start | bytes 6148
  385.7 8.2 %slice-start = ((s8[6291456]{0:T(1024)(128)(4,1)}), s8[4194304]{0:T(1024)(128)(4,1)S(1)}, s32[]{:S(2)}) async-start(s8[6291456]{0:T(1024)(128)(4,1)} %bitcast.5), calls=%async_computation.6 | async-start | bytes 8388608
  387.8 6.1 %slice-start.1 = ((s8[6291456]{0:T(1024)(128)(4,1)}), s8[2097152]{0:T(1024)(128)(4,1)S(1)}, s32[]{:S(2)}) async-start(s8[6291456]{0:T(1024)(128)(4,1)} %bitcast.5), calls=%async_computation.7 | async-start | bytes 4194304
  387.8 8.9 %slice-start.2 = ((s8[6291456]{0:T(1024)(128)(4,1)}), s8[4194304]{0:T(1024)(128)(4,1)S(1)}, s32[]{:S(2)}) async-start(s8[6291456]{0:T(1024)(128)(4,1)} %bitcast.7), calls=%async_computation.8 | async-start | bytes 8388608
  393.9 3.1 slice-start.3
Sparse Core Ops, SparseCore 0:
  9.5 25.2 all-gather.4
  37.6 98.6 all-gather.6
  139.1 96.8 all-gather.8
  238.6 96.8 all-gather.10
  349.3 29.3 reduce-scatter.1
where the time goes:
time: 407 us; the launch traced here: 406 us
  waiting for transfers between devices  342 us (84%)
  matrix products  22.2 us (5%)
  between operations  13.8 us (3%)
  local copies, waits for them, and re-layouts  11.9 us (3%)
  other arithmetic  9.99 us (2%)
  blocking collectives  5.76 us (1%)
    all_gather x1, waiting for transfers between devices, shards(): lax.all_gather(down_local, 'fs', axis=0, tiled=True)  99.5 us
    all_gather x1, waiting for transfers between devices, shards(): lax.all_gather(gate_local, 'fs', axis=0, tiled=True)  99.4 us
    all_gather x1, waiting for transfers between devices, shards(): lax.all_gather(up_local, 'fs', axis=0, tiled=True)  91.1 us
    reduce_scatter x1, waiting for transfers between devices, shards(): lax.psum_scatter(partial_value.astype(jnp.bfloat16), 'tp', scatter_dimens...  29.5 us
    all_gather x1, waiting for transfers between devices, shards(): whole = lax.all_gather(tokens, 'tp', axis=1, tiled=True)  21.5 us
    dot_general x1, matrix products, shards(): lax.dot_general(hidden, down_full, contract, preferred_element_type=jnp.f...  13.6 us
    unnamed x17, local copies, waits for them, and re-layouts  11.9 us
    dot_general x1, matrix products, shards(): gate = jnp.dot(normalized, gate_full, preferred_element_type=jnp.float32)  8.54 us
  transfers between devices with their start and end apart: 5, of which 5 were waited for; matrix products, arithmetic and copies ran while one was open for 4% of the time, Pallas kernels for 0%

commit v1 on v0

--- a/solution.py
+++ b/solution.py
@@ -10,7 +10,13 @@
     gate_local = (pre_gain[:, None] * gate_weight).astype(jnp.bfloat16)
     up_local = (pre_gain[:, None] * up_weight).astype(jnp.bfloat16)
     down_local = down_weight.astype(jnp.bfloat16)
-    whole = lax.all_gather(tokens, "tp", axis=1, tiled=True)
+    size = lax.axis_size("tp")
+    moving, blocks = (tokens, [tokens])
+    for _ in range(size - 1):
+        moving = lax.ppermute(moving, "tp", [(i, (i + 1) % size) for i in range(size)])
+        blocks.insert(0, moving)
+    merged = jnp.concatenate(blocks, axis=1)
+    whole = jnp.roll(merged, (lax.axis_index("tp") + 1) * tokens.shape[1], axis=1)
     widened = whole.astype(jnp.float32)
     width = whole.shape[1]
     normalized = (

time: 407 us -> 383 us (0.941)
  waiting for transfers between devices: 342 us -> 317 us
    all_gather x1, waiting for transfers between devices: 99.4 us -> 70.1 us  [shards(): lax.all_gather(gate_local, 'fs', axis=0, tiled=True)]
    ppermute x0 -> x3, waiting for transfers between devices: none -> 26 us  [shards(): lax.ppermute(moving, 'tp', [(i, (i + 1) % size) for i in range(size)])]
    all_gather x1 -> x0, waiting for transfers between devices: 21.5 us -> none  [shards(): whole = lax.all_gather(tokens, 'tp', axis=1, tiled=True)]
    unnamed x17 -> x26, local copies, waits for them, and re-layouts: 11.9 us -> 14.3 us
  transfers between devices with their start and end apart: 5 -> 7, of which waited for: 5 -> 7; matrix products, arithmetic and copies ran while one was open for 4% -> 3% of each run, Pallas kernels for 0% -> 0%
where the time goes in v1:
time: 383 us
  waiting for transfers between devices  317 us (83%)
  matrix products  22.7 us (6%)
  local copies, waits for them, and re-layouts  14.4 us (4%)
  between operations  13.9 us (4%)
  other arithmetic  8.44 us (2%)
  blocking collectives  5.76 us (2%)
    all_gather x1, waiting for transfers between devices, shards(): lax.all_gather(down_local, 'fs', axis=0, tiled=True)  99.7 us
    all_gather x1, waiting for transfers between devices, shards(): lax.all_gather(up_local, 'fs', axis=0, tiled=True)  90.5 us
    all_gather x1, waiting for transfers between devices, shards(): lax.all_gather(gate_local, 'fs', axis=0, tiled=True)  70.1 us
    reduce_scatter x1, waiting for transfers between devices, shards(): lax.psum_scatter(partial_value.astype(jnp.bfloat16), 'tp', scatter_dimens...  29.5 us
    ppermute x3, waiting for transfers between devices, shards(): lax.ppermute(moving, 'tp', [(i, (i + 1) % size) for i in range(size)])  26 us
    unnamed x26, local copies, waits for them, and re-layouts  14.3 us
    dot_general x1, matrix products, shards(): lax.dot_general(hidden, down_full, contract, preferred_element_type=jnp.f...  14.2 us
    dot_general x1, matrix products, shards(): gate = jnp.dot(normalized, gate_full, preferred_element_type=jnp.float32)  8.54 us
  transfers between devices with their start and end apart: 7, of which 7 were waited for; matrix products, arithmetic and copies ran while one was open for 3% of the time, Pallas kernels for 0%

profile of v1, /device:TPU:0, one launch (start us, length us, event | category | flops | bytes accessed | tf_op | source)
XLA Modules:
  0.0 382.5 jit_solution(4125927931957891744)
XLA Ops:
  7.2 0.0 copy-start.2
  7.2 0.0 copy-start
  7.2 0.0 all-gather.4.cloned.1.call-start
  7.2 3.6 multiply_convert_fusion.1
  10.8 0.0 all-gather.4.cloned.1.call-update
  10.8 0.0 all-gather.6.cloned.1.call-start
  10.9 0.7 all-gather.6.cloned.1.call-update
  11.6 0.0 all-gather.8.cloned.1.call-start
  11.6 0.0 copy-done.2
  11.7 1.0 convert_element_type.32
  12.6 0.0 all-gather.8.cloned.1.call-update
  12.6 0.0 reduce-scatter.2.cloned.1.call-start
  12.7 0.0 copy-done
  12.7 0.5 collective-permute-start
  13.2 8.8 %collective-permute-done = bf16[512,512]{1,0:T(8,128)(2,1)S(1)} collective-permute-done((bf16[512,512]{1,0:T(8,128)(2,1)S(1)}, bf16[512,512]{1,0:T(8,128)(2,1)S(1)}, u32[]{:S(2)}, u32[]{:S(2)}) %collective-permute-start) | collective-permute-done | bytes 524320 | tf_op jit(solution)/shard_map/ppermute | solution.py:16
  22.1 0.0 collective-permute-start.1
  22.1 8.6 %collective-permute-done.1 = bf16[512,512]{1,0:T(8,128)(2,1)S(1)} collective-permute-done((bf16[512,512]{1,0:T(8,128)(2,1)S(1)}, bf16[512,512]{1,0:T(8,128)(2,1)S(1)}, u32[]{:S(2)}, u32[]{:S(2)}) %collective-permute-start.1) | collective-permute-done | bytes 524320 | tf_op jit(solution)/shard_map/ppermute | solution.py:16
  30.7 0.0 collective-permute-start.2
  30.7 8.6 %collective-permute-done.2 = bf16[512,512]{1,0:T(8,128)(2,1)S(1)} collective-permute-done((bf16[512,512]{1,0:T(8,128)(2,1)S(1)}, bf16[512,512]{1,0:T(8,128)(2,1)S(1)}, u32[]{:S(2)}, u32[]{:S(2)}) %collective-permute-start.2) | collective-permute-done | bytes 524320 | tf_op jit(solution)/shard_map/ppermute | solution.py:16
  39.3 0.1 constant_dynamic-update-slice_fusion.7
  39.3 0.1 constant_dynamic-update-slice_fusion.6
  39.4 0.1 constant_dynamic-update-slice_fusion.5
  39.5 0.1 constant_dynamic-update-slice_fusion.4
  39.5 0.1 constant_dynamic-update-slice_fusion.3
  39.6 0.1 constant_dynamic-update-slice_fusion.2
  39.7 0.1 constant_dynamic-update-slice_fusion.1
  39.7 0.1 constant_dynamic-update-slice_fusion
  39.8 0.0 copy-start.1
  39.8 2.0 copy-done.1
  41.8 0.5 fusion
  42.3 70.1 %all-gather.4.cloned.1.call-done = bf16[2048,1536]{1,0:T(8,128)(2,1)} async-done(((bf16[256,1536]{1,0:T(8,128)(2,1)}), bf16[2048,1536]{1,0:T(8,128)(2,1)}) %all-gather.4.cloned.1.call-update) | async-done | bytes 6291472 | tf_op jit(solution)/shard_map/all_gather | solution.py:27
  112.4 8.5 %fusion.8 = f32[512,1536]{1,0:T(8,128)} fusion(bf16[2048,1536]{1,0:T(8,128)(2,1)} %all-gather.4.cloned.1.call-done, f32[512]{0:T(512)S(1)} %add_rsqrt_fusion.1, bf16[512,4096]{1,0:T(8,128)(2,1)} %copy-done.1, s32[]{:T(128)S(6)} %select_n.14), kind=kOutput, calls=%fused_computation.14 | convolution fusion | flops 3224371200 | bytes 11536388 | tf_op jit(solution)/shard_map/dot_general | solution.py:31
  120.9 0.0 copy-start.3
  121.0 90.5 %all-gather.6.cloned.1.call-done = bf16[2048,1536]{1,0:T(8,128)(2,1)} async-done(((bf16[256,1536]{1,0:T(8,128)(2,1)}), bf16[2048,1536]{1,0:T(8,128)(2,1)}) %all-gather.6.cloned.1.call-update) | async-done | bytes 6291472 | tf_op jit(solution)/shard_map/all_gather | solution.py:28
  211.5 99.7 %all-gather.8.cloned.1.call-done = bf16[2048,1536]{1,0:T(8,128)(2,1)} async-done(((bf16[256,1536]{1,0:T(8,128)(2,1)}), bf16[2048,1536]{1,0:T(8,128)(2,1)}) %all-gather.8.cloned.1.call-update) | async-done | bytes 6291472 | tf_op jit(solution)/shard_map/all_gather | solution.py:29
  311.2 14.2 %convolution_convert_fusion = bf16[512,2048]{1,0:T(8,128)(2,1)} fusion(bf16[2048,1536]{1,0:T(8,128)(2,1)} %all-gather.8.cloned.1.call-done, bf16[2048,1536]{1,0:T(8,128)(2,1)} %all-gather.6.cloned.1.call-done, f32[512,1536]{1,0:T(8,128)} %fusion.8, f32[512]{0:T(512)S(1)} %add_rsqrt_fusion.1, bf16[512,4096]{1,0:T(8,128)(2,1)} %copy-done.1, s32[]{:T(128)S(6)} %select_n.14), kind=kOutput, calls=%fused_computation.6 | convolution fusion | flops 6451363840 | bytes 19924996 | tf_op jit(solution)/shard_map/dot_general | solution.py:34
  325.4 0.0 reduce-scatter.2.cloned.1.call-update
  325.4 29.5 %reduce-scatter.2.cloned.1.call-done = bf16[512,512]{1,0:T(8,128)(2,1)} async-done(((bf16[512,2048]{1,0:T(8,128)(2,1)}), bf16[512,512]{1,0:T(8,128)(2,1)}) %reduce-scatter.2.cloned.1.call-update) | async-done | bytes 524304 | tf_op jit(solution)/shard_map/reduce_scatter | solution.py:35
  354.9 1.2 fusion.3
  356.1 5.8 %psum.7 = f32[512,1]{0,1:T(1,128)S(1)} all-reduce(f32[512,1]{0,1:T(1,128)S(1)} %bitcast.10), channel_id=1, replica_groups=mesh['fs'=8,'tp'=4] {'tp'}, use_global_device_ids=true, to_apply=%region_3.4 | all-reduce | flops 512 | bytes 4096 | tf_op jit(solution)/shard_map/psum | solution.py:38
  361.9 0.0 copy-done.3
  361.9 0.0 slice-start
  361.9 2.2 fusion.5
  364.1 0.0 slice-start.1
  364.1 0.0 slice-start.2
  364.1 6.1 %copy.20 = bf16[2048,1536]{1,0:T(8,128)(2,1)} copy(bf16[2048,1536]{1,0:T(8,128)(2,1)} %all-gather.4.cloned.1.call-done) | data formatting | bytes 12582912
  370.2 0.0 slice-done
  370.2 0.0 slice-done.1
  370.2 0.0 slice-start.3
  370.2 2.8 copy.21
  373.0 0.0 slice-done.2
  373.0 0.3 slice-done.3
  373.3 2.7 copy.22
  (4 shorter events, 0.0 us)
Async XLA Ops:
  7.2 4.5 %copy-start.2 = (f32[256,1536]{1,0:T(8,128)S(1)}, f32[256,1536]{1,0:T(8,128)}, u32[]{:S(2)}) copy-start(f32[256,1536]{1,0:T(8,128)} %param.10) | copy-start | bytes 4718596
  7.2 5.5 %copy-start = (bf16[512,512]{1,0:T(8,128)(2,1)S(1)}, bf16[512,512]{1,0:T(8,128)(2,1)}, u32[]{:S(2)}) copy-start(bf16[512,512]{1,0:T(8,128)(2,1)} %param.6) | copy-start | bytes 1572868
  7.2 105.2 %all-gather.4.cloned.1.call-start = ((), (), s32[]{:S(2)}) async-start(), calls=%async_computation.1 | async-start | bytes 7077888 | tf_op jit(solution)/shard_map/all_gather | solution.py:27
  10.8 200.7 %all-gather.6.cloned.1.call-start = ((), (), s32[]{:S(2)}) async-start(), calls=%async_computation.2 | async-start | bytes 7077888 | tf_op jit(solution)/shard_map/all_gather | solution.py:28
  11.6 299.6 %all-gather.8.cloned.1.call-start = ((), (), s32[]{:S(2)}) async-start(), calls=%async_computation.3 | async-start | bytes 7077888 | tf_op jit(solution)/shard_map/all_gather | solution.py:29
  12.6 342.3 %reduce-scatter.2.cloned.1.call-start = ((), (), s32[]{:S(2)}) async-start(), calls=%async_computation.4 | async-start | bytes 2621440 | tf_op jit(solution)/shard_map/reduce_scatter | solution.py:35
  12.7 9.4 %collective-permute-start = (bf16[512,512]{1,0:T(8,128)(2,1)S(1)}, bf16[512,512]{1,0:T(8,128)(2,1)S(1)}, u32[]{:S(2)}, u32[]{:S(2)}) collective-permute-start(bf16[512,512]{1,0:T(8,128)(2,1)S(1)} %copy-done), channel_id=1, source_target_pairs={{0,1},{1,2},{2,3},{3,0},{4,5},{5,6},{6,7},{7,4},{8,9},{9,10},{10,1... | collective-permute-start | bytes 1572872 | tf_op jit(solution)/shard_map/ppermute | solution.py:16
  22.1 8.6 %collective-permute-start.1 = (bf16[512,512]{1,0:T(8,128)(2,1)S(1)}, bf16[512,512]{1,0:T(8,128)(2,1)S(1)}, u32[]{:S(2)}, u32[]{:S(2)}) collective-permute-start(bf16[512,512]{1,0:T(8,128)(2,1)S(1)} %collective-permute-done), channel_id=1, source_target_pairs={{0,1},{1,2},{2,3},{3,0},{4,5},{5,6},{6,7},{7,4},{8,9},{9,10},{10,1... | collective-permute-start | bytes 1572872 | tf_op jit(solution)/shard_map/ppermute | solution.py:16
  30.7 8.6 %collective-permute-start.2 = (bf16[512,512]{1,0:T(8,128)(2,1)S(1)}, bf16[512,512]{1,0:T(8,128)(2,1)S(1)}, u32[]{:S(2)}, u32[]{:S(2)}) collective-permute-start(bf16[512,512]{1,0:T(8,128)(2,1)S(1)} %collective-permute-done.1), channel_id=1, source_target_pairs={{0,1},{1,2},{2,3},{3,0},{4,5},{5,6},{6,7},{7,4},{8,9},{9,10},{10,1... | collective-permute-start | bytes 1572872 | tf_op jit(solution)/shard_map/ppermute | solution.py:16
  39.8 2.0 copy-start.1
  120.9 241.0 %copy-start.3 = (f32[512]{0:T(512)S(1)}, f32[512]{0:T(512)}, u32[]{:S(2)}) copy-start(f32[512]{0:T(512)} %param.11) | copy-start | bytes 6148
  361.9 8.2 %slice-start = ((s8[6291456]{0:T(1024)(128)(4,1)}), s8[4194304]{0:T(1024)(128)(4,1)S(1)}, s32[]{:S(2)}) async-start(s8[6291456]{0:T(1024)(128)(4,1)} %bitcast.5), calls=%async_computation.5 | async-start | bytes 8388608
  364.1 6.1 %slice-start.1 = ((s8[6291456]{0:T(1024)(128)(4,1)}), s8[2097152]{0:T(1024)(128)(4,1)S(1)}, s32[]{:S(2)}) async-start(s8[6291456]{0:T(1024)(128)(4,1)} %bitcast.5), calls=%async_computation.6 | async-start | bytes 4194304
  364.1 8.9 %slice-start.2 = ((s8[6291456]{0:T(1024)(128)(4,1)}), s8[4194304]{0:T(1024)(128)(4,1)S(1)}, s32[]{:S(2)}) async-start(s8[6291456]{0:T(1024)(128)(4,1)} %bitcast.7), calls=%async_computation.7 | async-start | bytes 8388608
  370.2 3.1 slice-start.3
Sparse Core Ops, SparseCore 0:
  11.0 101.3 all-gather.3
  114.6 96.8 all-gather.5
  214.3 96.8 all-gather.7
  325.5 29.3 reduce-scatter.1
